TPU v7x, 32 devices: a whole 2x2x4 slice. The times are simulated.
32 devices in a mesh: rep: 2 (over x), fs: 4 (over z), tp: 4 (over y, core).
Axes of the slice: x: 2, y: 2, z: 4, core: 2. Of those that a mesh axis runs over, the one named last changes fastest.
Arguments:
- tokens: bfloat16 [8192, 2048], P(('rep', 'fs'), 'tp'), may hold values from -6 to 6
- mix_gain: float32 [2048], replicated, may hold values from 0.1 to 1.9
- query_weight: bfloat16 [2048, 512], P('fs', 'tp'), may hold values from -0.125 to 0.125
- key_weight: bfloat16 [2048, 512], P('fs', 'tp'), may hold values from -0.125 to 0.125
- value_weight: bfloat16 [2048, 1024], P('fs', 'tp'), may hold values from -0.125 to 0.125
- gate_weight: bfloat16 [2048, 1024], P('fs', 'tp'), may hold values from -0.125 to 0.125
- out_weight: bfloat16 [1024, 2048], P('tp', 'fs'), may hold values from -0.1875 to 0.1875
- head_gain: float32 [8, 128], P('tp'), may hold values from 0.1 to 1.9
- ffn_gain: float32 [2048], replicated, may hold values from 0.1 to 1.9
- ffn_gate: bfloat16 [2048, 5632], P('fs', 'tp'), may hold values from -0.125 to 0.125
- ffn_up: bfloat16 [2048, 5632], P('fs', 'tp'), may hold values from -0.125 to 0.125
- ffn_down: bfloat16 [5632, 2048], P('tp', 'fs'), may hold values from -0.078125 to 0.078125
Outputs:
- layer_out: bfloat16 [8192, 2048], P(('rep', 'fs'), 'tp')
All inputs are finite; a program needn't handle non-finite values.
Results may differ from a plain program's by a relative error of at most 0.03.
Values may be sent and summed in bfloat16 or wider, within the bound.
A program may use at most 128 MiB of HBM per device.

v0:
```python
import jax
import jax.numpy as jnp
import numpy as np
from jax import lax
from jax.experimental import pallas as pl
from jax.experimental.pallas import tpu as pltpu
from jax.sharding import PartitionSpec as P

HEADS = 8
DK = 64
DV = 128
BLOCK = 64
SEQ = 256


epsilon = 1e-06
rope_base = 10000.0


def norm_rows(values, gain_row):
    floats = values.astype(jnp.float32)
    scaled = floats * lax.rsqrt(jnp.mean(floats * floats, axis=-1, keepdims=True) + epsilon)
    return (scaled * gain_row).astype(jnp.bfloat16)


def rotate(values, positions):
    half_dim = values.shape[-1] // 2
    frequency = rope_base ** (-jnp.linspace(0.0, 1.0, half_dim, dtype=jnp.float32))
    angles = positions.astype(jnp.float32)[:, None] * frequency[None, :]
    cosine = jnp.cos(angles)[:, None, :]
    sine_part = jnp.sin(angles)[:, None, :]
    paired = values.reshape(values.shape[:-1] + (half_dim, 2))
    leading = paired[..., 0]
    trailing = paired[..., 1]
    turned = jnp.stack(
        [leading * cosine - trailing * sine_part, leading * sine_part + trailing * cosine], axis=-1
    )
    return turned.reshape(values.shape)


def log_decay(head_index, total_heads):
    return jnp.log1p(-jnp.exp2(-5.0 - 4.0 * head_index.astype(jnp.float32) / (total_heads - 1)))


def retention(queries, key_rows, value_rows, decay_rates):
    highest = lax.Precision.HIGHEST
    row_count, head_count = (queries.shape[0], queries.shape[1])
    seq_count = row_count // SEQ
    block_count = SEQ // BLOCK

    def to_blocks(values):
        shaped = values.reshape((seq_count, block_count, BLOCK) + values.shape[1:])
        return jnp.moveaxis(shaped, 1, 0)

    inside = jnp.arange(BLOCK, dtype=jnp.int32)
    gap = (inside[:, None] - inside[None, :]).astype(jnp.float32)
    within_mask = jnp.where(
        gap[None] >= 0.0, jnp.exp(jnp.maximum(gap, 0.0)[None] * decay_rates[:, None, None]), 0.0
    )
    query_scale = jnp.exp((inside + 1).astype(jnp.float32)[:, None] * decay_rates[None, :])
    key_scale = jnp.exp((BLOCK - 1 - inside).astype(jnp.float32)[:, None] * decay_rates[None, :])
    block_decay = jnp.exp(BLOCK * decay_rates)

    def advance(state, inputs):
        query_blk, key_blk, value_blk = inputs
        scores = (
            jnp.einsum("sihd,sjhd->shij", query_blk, key_blk, precision=highest) * within_mask[None]
        )
        local_part = jnp.einsum("shij,sjhv->sihv", scores, value_blk, precision=highest)
        carried = jnp.einsum(
            "sihd,shdv->sihv", query_blk * query_scale[None, :, :, None], state, precision=highest
        )
        update = jnp.einsum(
            "sjhd,sjhv->shdv", key_blk * key_scale[None, :, :, None], value_blk, precision=highest
        )
        return (block_decay[None, :, None, None] * state + update, local_part + carried)

    state_zero = jnp.zeros((seq_count, head_count, DK, DV), jnp.float32)
    _, outputs = lax.scan(
        advance, state_zero, (to_blocks(queries), to_blocks(key_rows), to_blocks(value_rows))
    )
    return jnp.moveaxis(outputs, 0, 1).reshape(row_count, head_count, DV)


def per_device_plain(
    tokens,
    mix_gain,
    query_weight,
    key_weight,
    value_weight,
    gate_weight,
    out_weight,
    head_gain,
    ffn_gain,
    ffn_gate,
    ffn_up,
    ffn_down,
):
    whole_rows = lax.all_gather(tokens, "tp", axis=1, tiled=True)
    row_count = whole_rows.shape[0]
    normed = norm_rows(whole_rows, mix_gain)
    pieces = (
        lax.all_gather(query_weight, "fs", axis=0, tiled=True),
        lax.all_gather(key_weight, "fs", axis=0, tiled=True),
        lax.all_gather(value_weight, "fs", axis=0, tiled=True),
        lax.all_gather(gate_weight, "fs", axis=0, tiled=True),
    )
    query_acc, key_acc, value_acc, gate_acc = tuple(
        (
            jnp.dot(normed, weight_piece, preferred_element_type=jnp.float32)
            for weight_piece in pieces
        )
    )
    heads_here = query_weight.shape[1] // DK
    positions = jnp.arange(row_count, dtype=jnp.int32) % SEQ
    queries = rotate(
        query_acc.astype(jnp.bfloat16).astype(jnp.float32).reshape(row_count, heads_here, DK),
        positions,
    )
    key_rows = rotate(
        key_acc.astype(jnp.bfloat16).astype(jnp.float32).reshape(row_count, heads_here, DK),
        positions,
    ) * DK ** (-0.5)
    value_rows = (
        value_acc.astype(jnp.bfloat16).astype(jnp.float32).reshape(row_count, heads_here, DV)
    )
    gate_rows = gate_acc.astype(jnp.bfloat16).astype(jnp.float32)
    first_head = lax.axis_index("tp") * heads_here
    decay_rates = log_decay(first_head + jnp.arange(heads_here, dtype=jnp.int32), HEADS)
    retained = retention(queries, key_rows, value_rows, decay_rates)
    center = jnp.mean(retained, axis=-1, keepdims=True)
    spread = jnp.mean(jnp.square(retained - center), axis=-1, keepdims=True)
    grouped = (retained - center) * lax.rsqrt(spread + epsilon) * head_gain[None]
    mixed = (grouped.reshape(row_count, heads_here * DV) * jax.nn.silu(gate_rows)).astype(
        jnp.bfloat16
    )
    mixer_terms = jnp.dot(
        mixed,
        lax.all_gather(out_weight, "fs", axis=1, tiled=True),
        preferred_element_type=jnp.float32,
    )
    mixer_share = lax.psum_scatter(
        mixer_terms.astype(jnp.bfloat16), "tp", scatter_dimension=1, tiled=True
    ).astype(jnp.float32)
    resid_shard = (tokens.astype(jnp.float32) + mixer_share).astype(jnp.bfloat16)
    resid_whole = lax.all_gather(resid_shard, "tp", axis=1, tiled=True)
    normed_ffn = norm_rows(resid_whole, ffn_gain)

    def add_rows(weight_piece):
        return jnp.dot(normed_ffn, weight_piece, preferred_element_type=jnp.float32)

    gate_hidden = add_rows(lax.all_gather(ffn_gate, "fs", axis=0, tiled=True))
    up_hidden = add_rows(lax.all_gather(ffn_up, "fs", axis=0, tiled=True))
    hidden = (jax.nn.silu(gate_hidden) * up_hidden).astype(jnp.bfloat16)
    ffn_terms = jnp.dot(
        hidden,
        lax.all_gather(ffn_down, "fs", axis=1, tiled=True),
        preferred_element_type=jnp.float32,
    )
    ffn_share = lax.psum_scatter(
        ffn_terms.astype(jnp.bfloat16), "tp", scatter_dimension=1, tiled=True
    ).astype(jnp.float32)
    return (resid_shard.astype(jnp.float32) + ffn_share).astype(jnp.bfloat16)


MESH = pl.DeviceIdType.MESH
LANES = 128


def fused_kernel(
    tokens_ref, mix_gain_ref, query_ref, key_ref, value_ref, gate_ref, proj_out_ref, head_gain_ref,
    ffn_gain_ref, ffn_gate_ref, ffn_up_ref, ffn_down_ref, cos_ref, sin_ref, rate_ref,
    out_ref,
    w_mix, w_out, w_ffn, w_down, x_all, res_all, normed, normed_ffn, proj, mixed, hidden, mask,
    corner1, corner1_in, beside1, beside1_in, across1, across1_in, own1,
    corner2, corner2_in, beside2, beside2_in, across2, across2_in, own2,
    local_sem, z_send, z_recv, x_send, x_recv, y_send, y_recv,
):
    f32, bf16 = jnp.float32, jnp.bfloat16
    rep, here, tp = lax.axis_index("rep"), lax.axis_index("fs"), lax.axis_index("tp")
    core, chip = tp % 2, tp // 2
    beside_id, across_id, corner_id = tp + 1 - 2 * core, (tp + 2) % 4, 3 - tp
    rows, width = tokens_ref.shape
    seqs = rows // SEQ
    shard = query_ref.shape[0]
    key_width, value_width = query_ref.shape[1], value_ref.shape[1]
    heads = head_gain_ref.shape[0]
    ffn_blocks = ffn_gate_ref.shape[1] // LANES
    down_chunks = ffn_down_ref.shape[1] // LANES
    pair_width = 2 * LANES

    def own_rows(size, base=None):
        index = here if base is None else base
        return pl.ds(pl.multiple_of(index * size, size), size)

    local = []

    def bring(source, target):
        copy = pltpu.make_async_copy(source, target, local_sem.at[len(local)])
        copy.start()
        local.append(copy)
        return copy

    token_columns = own_rows(width, tp)
    bring_tokens = bring(tokens_ref, x_all.at[:, token_columns])
    bring_mix = []
    start = 0
    for ref in (query_ref, key_ref, value_ref, gate_ref):
        bring_mix.append(bring(ref, w_mix.at[own_rows(shard), pl.ds(start, ref.shape[1])]))
        start += ref.shape[1]
    bring_out = bring(proj_out_ref, w_out.at[:, own_rows(proj_out_ref.shape[1])])
    bring_ffn = []
    for block in range(ffn_blocks):
        pair = []
        for part, ref in enumerate((ffn_gate_ref, ffn_up_ref)):
            pair.append(
                bring(
                    ref.at[:, pl.ds(block * LANES, LANES)],
                    w_ffn.at[own_rows(shard), pl.ds(block * pair_width + part * LANES, LANES)],
                )
            )
        bring_ffn.append(pair)
    bring_down = [
        bring(ffn_down_ref.at[:, pl.ds(c * LANES, LANES)], w_down.at[c, :, own_rows(LANES)])
        for c in range(down_chunks)
    ]

    chunks = []
    mix_chunks = w_mix.shape[1] // pair_width
    half_shard = shard // 2

    def row_chunk(buffer, column):
        def view(s, half):
            first = pl.multiple_of(s * shard + half * half_shard, half_shard)
            return buffer.at[pl.ds(first, half_shard), pl.ds(column, pair_width)]

        return view

    for i in range(mix_chunks):
        needs = {0: bring_mix[:2], 1: bring_mix[2:3], 2: bring_mix[3:]}[i]
        chunks.append((row_chunk(w_mix, i * pair_width), needs))

    def out_view(s, half):
        size, columns = w_out.shape[0] // 2, proj_out_ref.shape[1]
        return w_out.at[own_rows(size, half), own_rows(columns, s)]

    chunks.append((out_view, [bring_out]))
    for block in range(ffn_blocks):
        chunks.append((row_chunk(w_ffn, block * pair_width), bring_ffn[block]))

    def down_view(c):
        def view(s, half):
            size = w_down.shape[1] // 2
            return w_down.at[c, own_rows(size, half), own_rows(LANES, s)]

        return view

    for c in range(down_chunks):
        chunks.append((down_view(c), [bring_down[c]]))
    total = len(chunks)
    first_ffn = mix_chunks + 1
    first_down = first_ffn + ffn_blocks

    barrier = pltpu.get_barrier_semaphore()
    for target in (
        {"fs": (here + 1) % 4}, {"fs": (here + 3) % 4}, {"rep": 1 - rep}, {"tp": beside_id}, {"tp": across_id},
    ):
        pl.semaphore_signal(barrier, inc=1, device_id=target, device_id_type=MESH)
    pl.semaphore_wait(barrier, 5)

    def z_copy(k, d, hop, s, target):
        view = chunks[k][0](s, rep)
        return pltpu.make_async_remote_copy(
            src_ref=view, dst_ref=view, send_sem=z_send.at[k, d, hop - 1], recv_sem=z_recv.at[k, d, hop - 1],
            device_id={"fs": target}, device_id_type=MESH,
        )

    def x_copy(k, d, hop, s, half):
        view = chunks[k][0](s, half)
        return pltpu.make_async_remote_copy(
            src_ref=view, dst_ref=view, send_sem=x_send.at[k, d, hop - 1], recv_sem=x_recv.at[k, d, hop - 1],
            device_id={"rep": 1 - rep}, device_id_type=MESH,
        )

    pending = {}

    def z_send_start(step, k, d, hop, guard):
        s = here - (hop - 1) if d == 0 else here + (hop - 1)
        target = here + 1 if d == 0 else here - 1

        @pl.when(guard)
        def _():
            z_copy(k, d, hop, s, target).start()

        def finish():
            @pl.when(guard)
            def _():
                z_copy(k, d, hop, s, target).wait_send()

        pending.setdefault(step, []).append(finish)

    def own_send(step, k):
        for copy in chunks[k][1]:
            copy.wait()
        z_send_start(step, k, 0, 1, here <= 2)
        z_send_start(step, k, 1, 1, here >= 1)

    def arrive(step, k, d, hop):
        s = here - hop if d == 0 else here + hop
        origin = here - 1 if d == 0 else here + 1
        valid = here >= hop if d == 0 else here + hop <= 3

        @pl.when(valid)
        def _():
            z_copy(k, d, hop, s, origin).wait_recv()

        if hop < 3:
            onward = here <= 2 if d == 0 else here >= 1
            z_send_start(step, k, d, hop + 1, jnp.logical_and(valid, onward))

        @pl.when(valid)
        def _():
            x_copy(k, d, hop, s, rep).start()

        def finish():
            @pl.when(valid)
            def _():
                x_copy(k, d, hop, s, rep).wait_send()

        pending.setdefault(step, []).append(finish)

    def x_arrive(k, d, hop):
        s = here - hop if d == 0 else here + hop
        valid = here >= hop if d == 0 else here + hop <= 3

        @pl.when(valid)
        def _():
            x_copy(k, d, hop, s, 1 - rep).wait_recv()

    def finish_sends(step):
        for finish in pending.pop(step, ()):
            finish()

    def advance(step):
        finish_sends(step - 2)
        if step == 0:
            own_send(0, 0)
        if step + 1 < total:
            own_send(step, step + 1)
        for hop in (1, 2, 3):
            k = step - hop + 1
            if 0 <= k < total:
                for d in (0, 1):
                    arrive(step, k, d, hop)
        for hop in (1, 2, 3):
            k = step - hop
            if 0 <= k < total:
                for d in (0, 1):
                    x_arrive(k, d, hop)

    y_index = {}
    for name in ("gather1", "gather2", "reduce1"):
        for leg in ("beside", "across", "corner"):
            y_index[name, leg] = len(y_index) * seqs
    for leg in ("beside", "across", "corner"):
        y_index["reduce2", leg] = 9 * seqs + (len(y_index) - 9) * seqs * down_chunks

    def y_copy(name, leg, index, source, target, to):
        slot = y_index[name, leg] + index
        return pltpu.make_async_remote_copy(
            src_ref=source, dst_ref=target, send_sem=y_send.at[slot], recv_sem=y_recv.at[slot],
            device_id={"tp": to}, device_id_type=MESH,
        )

    def seq_rows(j):
        return pl.ds(j * SEQ, SEQ)

    def gather_copy(name, buffer, leg, j, arriving):
        to = across_id if leg == "across" else beside_id
        source_of = {"beside": (tp, beside_id), "across": (tp, across_id), "corner": (across_id, corner_id)}
        owner = source_of[leg][1 if arriving else 0]
        view = buffer.at[seq_rows(j), own_rows(width, owner)]
        return y_copy(name, leg, j, view, view, to)

    y_pending = []

    def gather_send(name, buffer, leg, j):
        copy = gather_copy(name, buffer, leg, j, False)
        copy.start()
        y_pending.append(copy)

    def gather_wait(name, buffer, leg, j):
        gather_copy(name, buffer, leg, j, True).wait_recv()

    def relay(name, buffer, j):
        gather_wait(name, buffer, "across", j)
        gather_send(name, buffer, "corner", j)

    def norm_into(source, gain_ref, target, source_row, target_row):
        group = 16

        @pl.loop(0, SEQ // group)
        def _(i):
            offset = pl.multiple_of(i * group, group)
            floats = source[pl.ds(source_row + offset, group), :].astype(f32)
            scale = lax.rsqrt(jnp.mean(floats * floats, axis=-1, keepdims=True) + epsilon)
            target[pl.ds(target_row + offset, group), :] = (floats * scale * gain_ref[...]).astype(bf16)

    def make_mask():
        gap = lax.broadcasted_iota(jnp.int32, (SEQ, SEQ), 0) - lax.broadcasted_iota(jnp.int32, (SEQ, SEQ), 1)
        positive = jnp.maximum(gap, 0).astype(f32)
        for head in range(heads):
            rate = rate_ref[pl.ds(tp * heads + head, 1), :]
            mask[head] = jnp.where(gap >= 0, jnp.exp(positive * rate), 0.0)

    def mix(j):
        gather_wait("gather1", x_all, "beside", j)
        gather_wait("gather1", x_all, "corner", j)
        norm_into(x_all, mix_gain_ref, normed, j * SEQ, 0)
        proj[...] = jnp.dot(normed[...], w_mix[...], preferred_element_type=f32).astype(bf16)
        highest = lax.Precision.HIGHEST
        lane = lax.broadcasted_iota(jnp.int32, (SEQ, key_width), 1)
        cosine, sine = cos_ref[...], sin_ref[...]

        def turn(values):
            following = pltpu.roll(values, key_width - 1, 1)
            preceding = pltpu.roll(values, 1, 1)
            other = jnp.where(lane % 2 == 0, -following, preceding)
            return values * cosine + other * sine

        query = turn(proj[:, :key_width].astype(f32))
        key = turn(proj[:, key_width : 2 * key_width].astype(f32)) * DK ** (-0.5)
        for head in range(heads):
            only = jnp.where(lane // DK == head, query, 0.0)
            scores = lax.dot_general(
                only, key, (((1,), (1,)), ((), ())), precision=highest, preferred_element_type=f32
            ) * mask[head]
            first = 2 * key_width + head * DV
            value = proj[:, first : first + DV].astype(f32)
            retained = jnp.dot(scores, value, precision=highest, preferred_element_type=f32)
            centered = retained - jnp.mean(retained, axis=-1, keepdims=True)
            spread = jnp.mean(centered * centered, axis=-1, keepdims=True)
            grouped = centered * lax.rsqrt(spread + epsilon) * head_gain_ref[head : head + 1, :]
            first += value_width
            gate = proj[:, first : first + DV].astype(f32)
            mixed[:, head * DV : (head + 1) * DV] = (grouped * jax.nn.silu(gate)).astype(bf16)

    def reduce_copy(name, leg, index, source, target):
        return y_copy(name, leg, index, source, target, across_id if leg == "across" else beside_id)

    def mix_reduce(j):
        def quarter(owner):
            return jnp.dot(mixed[...], w_out[:, own_rows(width, owner)], preferred_element_type=f32)

        def send(leg, source, target):
            copy = reduce_copy("reduce1", leg, j, source.at[j], target.at[j])
            copy.start()
            y_pending.append(copy)
            return copy

        corner1[j] = quarter(corner_id).astype(bf16)
        sent = send("corner", corner1, corner1_in)
        beside1[j] = quarter(beside_id).astype(bf16)
        send("beside", beside1, beside1_in)
        own1[j] = quarter(tp)
        far = quarter(across_id)
        sent.wait_recv()
        across1[j] = (far + corner1_in[j].astype(f32)).astype(bf16)
        send("across", across1, across1_in)

    def residual(j):
        reduce_copy("reduce1", "beside", j, beside1.at[j], beside1_in.at[j]).wait_recv()
        reduce_copy("reduce1", "across", j, across1.at[j], across1_in.at[j]).wait_recv()
        share = own1[j] + beside1_in[j].astype(f32) + across1_in[j].astype(f32)
        tokens = x_all[seq_rows(j), token_columns].astype(f32)
        res_all[seq_rows(j), token_columns] = (tokens + share).astype(bf16)
        gather_send("gather2", res_all, "across", j)
        gather_send("gather2", res_all, "beside", j)

    def ready(j):
        gather_wait("gather2", res_all, "beside", j)
        gather_wait("gather2", res_all, "corner", j)
        norm_into(res_all, ffn_gain_ref, normed_ffn, j * SEQ, j * SEQ)

    def ffn(first, last):
        @pl.loop(first, last)
        def _(b):
            weight_columns = own_rows(pair_width, b)
            hidden_columns = own_rows(LANES, b)

            @pl.loop(0, seqs)
            def _(j):
                part = own_rows(SEQ, j)
                both = jnp.dot(normed_ffn[part, :], w_ffn[:, weight_columns], preferred_element_type=f32)
                hidden[part, hidden_columns] = (jax.nn.silu(both[:, :LANES]) * both[:, LANES:]).astype(bf16)

    def reduce2(leg, c, j, source, target):
        part = own_rows(SEQ, j)
        return reduce_copy("reduce2", leg, c * seqs + j, source.at[c, part, :], target.at[c, part, :])

    def down(c):
        @pl.loop(0, seqs)
        def _(j):
            part = own_rows(SEQ, j)
            left = hidden[part, :]
            far = jnp.dot(left, w_down[c, :, own_rows(pair_width, 1 - chip)], preferred_element_type=f32)
            lower, upper = far[:, :LANES], far[:, LANES:]
            corner2[c, part, :] = jnp.where(core == 0, upper, lower).astype(bf16)
            sent = reduce2("corner", c, j, corner2, corner2_in)
            sent.start()
            onward = jnp.where(core == 0, lower, upper)
            near = jnp.dot(left, w_down[c, :, own_rows(pair_width, chip)], preferred_element_type=f32)
            lower, upper = near[:, :LANES], near[:, LANES:]
            beside2[c, part, :] = jnp.where(core == 0, upper, lower).astype(bf16)
            reduce2("beside", c, j, beside2, beside2_in).start()
            own2[c, part, :] = jnp.where(core == 0, lower, upper)
            sent.wait_recv()
            across2[c, part, :] = (onward + corner2_in[c, part, :].astype(f32)).astype(bf16)
            reduce2("across", c, j, across2, across2_in).start()

    def finish_down(c):
        @pl.loop(0, seqs)
        def _(j):
            part = own_rows(SEQ, j)
            reduce2("beside", c, j, beside2, beside2_in).wait_recv()
            reduce2("across", c, j, across2, across2_in).wait_recv()
            share = own2[c, part, :] + beside2_in[c, part, :].astype(f32) + across2_in[c, part, :].astype(f32)
            columns = pl.ds(pl.multiple_of(tp * width + c * LANES, LANES), LANES)
            kept = res_all[part, columns].astype(f32)
            out_ref[part, c * LANES : (c + 1) * LANES] = (kept + share).astype(bf16)
            for leg, source, target in (
                ("corner", corner2, corner2_in), ("beside", beside2, beside2_in), ("across", across2, across2_in),
            ):
                reduce2(leg, c, j, source, target).wait_send()

    work = {}

    def at(step, function, *args):
        work.setdefault(step, []).append((function, args))

    at(0, make_mask)
    for j in range(seqs):
        at(1 + j, relay, "gather1", x_all, j)
    mixed_at = mix_chunks + 2
    out_at = mixed_at + 1
    order = []
    for j in range(seqs):
        at(out_at + j + 3, ready, j)
    for j in range(seqs):
        at(out_at + j + 2, relay, "gather2", res_all, j)
    for j in range(seqs):
        at(out_at + j + 1, residual, j)
    for j in range(seqs):
        at(out_at + j, mix_reduce, j)
    for j in range(seqs):
        at(mixed_at + j, mix, j)
    done = 0
    ffn_from = out_at + seqs + 2
    for step in range(ffn_from, first_down + 3):
        there = min(ffn_blocks, step - first_ffn - 2)
        last = min(there, done + 4)
        if step == first_down + 2:
            last = ffn_blocks
        if last > done:
            at(step, ffn, done, last)
            done = last
    for c in range(down_chunks):
        at(first_down + 3 + c, down, c)
        if c:
            at(first_down + 3 + c, finish_down, c - 1)

    bring_tokens.wait()
    for j in range(seqs):
        gather_send("gather1", x_all, "across", j)
        gather_send("gather1", x_all, "beside", j)
    for step in range(total + 3):
        advance(step)
        for function, args in work.get(step, ()):
            function(*args)
    finish_down(down_chunks - 1)
    for step in sorted(pending):
        finish_sends(step)
    for copy in y_pending:
        copy.wait_send()


def layer(
    tokens, mix_gain, query_weight, key_weight, value_weight, gate_weight, out_weight, head_gain,
    ffn_gain, ffn_gate, ffn_up, ffn_down,
):
    bf16, f32 = jnp.bfloat16, jnp.float32
    rows, width = tokens.shape
    model = 4 * width
    seqs = rows // SEQ
    key_width, value_width = query_weight.shape[1], value_weight.shape[1]
    heads = head_gain.shape[0]
    mix_width = 2 * key_width + 2 * value_width
    hidden_width = ffn_gate.shape[1]
    blocks, down_chunks = hidden_width // LANES, ffn_down.shape[1] // LANES
    total = mix_width // (2 * LANES) + 1 + blocks + down_chunks
    frequency = rope_base ** (-np.linspace(0.0, 1.0, DK // 2))
    angles = np.arange(SEQ)[:, None] * frequency[None, :]
    cosine = np.tile(np.repeat(np.cos(angles), 2, axis=1), (1, heads)).astype(np.float32)
    sine = np.tile(np.repeat(np.sin(angles), 2, axis=1), (1, heads)).astype(np.float32)
    rates = np.log1p(-np.exp2(-5.0 - 4.0 * np.arange(HEADS) / (HEADS - 1)))
    rates = np.broadcast_to(rates[:, None], (HEADS, SEQ)).astype(np.float32)
    vmem, anywhere = pl.BlockSpec(memory_space=pltpu.VMEM), pl.BlockSpec(memory_space=pl.ANY)
    first_sum = [pltpu.VMEM((seqs, SEQ, width), bf16)] * 6
    second_sum = [pltpu.VMEM((down_chunks, rows, LANES), bf16)] * 6
    dma = pltpu.SemaphoreType.DMA
    return pl.pallas_call(
        fused_kernel,
        out_shape=jax.ShapeDtypeStruct((rows, width), bf16),
        in_specs=[anywhere, vmem] + [anywhere] * 5 + [vmem, vmem] + [anywhere] * 3 + [vmem] * 3,
        out_specs=vmem,
        scratch_shapes=[
            pltpu.VMEM((model, mix_width), bf16),
            pltpu.VMEM((out_weight.shape[0], model), bf16),
            pltpu.VMEM((model, 2 * hidden_width), bf16),
            pltpu.VMEM((down_chunks, hidden_width, 4 * LANES), bf16),
            pltpu.VMEM((rows, model), bf16),
            pltpu.VMEM((rows, model), bf16),
            pltpu.VMEM((SEQ, model), bf16),
            pltpu.VMEM((rows, model), bf16),
            pltpu.VMEM((SEQ, mix_width), bf16),
            pltpu.VMEM((SEQ, heads * DV), bf16),
            pltpu.VMEM((rows, hidden_width), bf16),
            pltpu.VMEM((heads, SEQ, SEQ), f32),
        ]
        + first_sum
        + [pltpu.VMEM((seqs, SEQ, width), f32)]
        + second_sum
        + [pltpu.VMEM((down_chunks, rows, LANES), f32)]
        + [
            dma((6 + 2 * blocks + down_chunks,)),
            dma((total, 2, 3)),
            dma((total, 2, 3)),
            dma((total, 2, 3)),
            dma((total, 2, 3)),
            dma((9 * seqs + 3 * seqs * down_chunks,)),
            dma((9 * seqs + 3 * seqs * down_chunks,)),
        ],
        compiler_params=pltpu.CompilerParams(
            collective_id=0, has_side_effects=True, vmem_limit_bytes=67043328
        ),
        name="layer",
    )(
        tokens, mix_gain.reshape(1, -1), query_weight, key_weight, value_weight, gate_weight, out_weight,
        head_gain, ffn_gain.reshape(1, -1), ffn_gate, ffn_up, ffn_down, cosine, sine, rates,
    )


def solution(mesh):
    shape = mesh.shape
    small = shape["rep"] == 2 and shape["fs"] == 4 and shape["tp"] == 4
    return jax.shard_map(
        layer if small else per_device_plain,
        mesh=mesh,
        in_specs=(
            P(("rep", "fs"), "tp"),
            P(),
            P("fs", "tp"),
            P("fs", "tp"),
            P("fs", "tp"),
            P("fs", "tp"),
            P("tp", "fs"),
            P("tp", None),
            P(),
            P("fs", "tp"),
            P("fs", "tp"),
            P("tp", "fs"),
        ),
        out_specs=P(("rep", "fs"), "tp"),
        check_vma=False,
    )
```

profile of v0, /device:TPU:0, one launch (start us, length us, event | category | flops | bytes accessed | tf_op | source)
XLA Modules:
  0.0 226.7 jit_solution(1657740131260508127)
XLA Ops:
  0.0 224.5 %layer.1 = bf16[1024,512]{1,0:T(8,128)(2,1)} custom-call(bf16[1024,512]{1,0:T(8,128)(2,1)} %tokens_ref.1, f32[1,2048]{1,0:T(1,128)} %bitcast.2, bf16[512,128]{1,0:T(8,128)(2,1)} %query_ref.1, bf16[512,128]{1,0:T(8,128)(2,1)} %key_ref.1, bf16[512,256]{1,0:T(8,128)(2,1)} %value_ref.1, bf16[512,256]{1,0:T(8,128)(2,1)} %gate_ref.1, ...), custom_call_target="tpu_custom_call" | custom-call | tf_op jit(solution)/shard_map/layer/pallas_call | solution.py:611
  224.5 2.3 copy.17
where the time goes:
time: 227 us
  Pallas kernels  224 us (99%)
    pallas_call x1, Pallas kernels, layer(): pl.pallas_call(fused_kernel, out_shape=jax.ShapeDtypeStruct((rows, width)...  224 us

commit v1 on v0

--- a/solution.py
+++ b/solution.py
@@ -165,6 +165,9 @@
 
 MESH = pl.DeviceIdType.MESH
 LANES = 128
+FFN_ROWS = 2
+FFN_PER_STEP = 3
+PLAN = ((0, 1, 3, 6, 10, 12), (2, 4, 5, 8, 14, 16), (5, 6, 7, 12, 18, 19), (8, 9, 11, 16, 20, 21))
 
 
 def fused_kernel(
@@ -173,8 +176,8 @@
     out_ref,
     w_mix, w_out, w_ffn, w_down, x_all, res_all, normed, normed_ffn, proj, mixed, hidden, mask,
     corner1, corner1_in, beside1, beside1_in, across1, across1_in, own1,
-    corner2, corner2_in, beside2, beside2_in, across2, across2_in, own2,
-    local_sem, z_send, z_recv, x_send, x_recv, y_send, y_recv,
+    corner2, corner2_in, beside2, beside2_in, across2, across2_in, own2, far2, sums, begun, result,
+    local_sem, z_send, z_recv, x_send, x_recv, y_send, y_recv, out_sem,
 ):
     f32, bf16 = jnp.float32, jnp.bfloat16
     rep, here, tp = lax.axis_index("rep"), lax.axis_index("fs"), lax.axis_index("tp")
@@ -193,35 +196,30 @@
         index = here if base is None else base
         return pl.ds(pl.multiple_of(index * size, size), size)
 
-    local = []
-
-    def bring(source, target):
-        copy = pltpu.make_async_copy(source, target, local_sem.at[len(local)])
-        copy.start()
-        local.append(copy)
-        return copy
+    def bring(slot, source, target):
+        return pltpu.make_async_copy(source, target, local_sem.at[slot])
 
     token_columns = own_rows(width, tp)
-    bring_tokens = bring(tokens_ref, x_all.at[:, token_columns])
+    bring_tokens = bring(0, tokens_ref, x_all.at[:, token_columns])
     bring_mix = []
     start = 0
     for ref in (query_ref, key_ref, value_ref, gate_ref):
-        bring_mix.append(bring(ref, w_mix.at[own_rows(shard), pl.ds(start, ref.shape[1])]))
+        bring_mix.append(bring(1 + len(bring_mix), ref, w_mix.at[own_rows(shard), pl.ds(start, ref.shape[1])]))
         start += ref.shape[1]
-    bring_out = bring(proj_out_ref, w_out.at[:, own_rows(proj_out_ref.shape[1])])
-    bring_ffn = []
-    for block in range(ffn_blocks):
-        pair = []
-        for part, ref in enumerate((ffn_gate_ref, ffn_up_ref)):
-            pair.append(
-                bring(
-                    ref.at[:, pl.ds(block * LANES, LANES)],
-                    w_ffn.at[own_rows(shard), pl.ds(block * pair_width + part * LANES, LANES)],
-                )
+    bring_out = bring(5, proj_out_ref, w_out.at[:, own_rows(proj_out_ref.shape[1])])
+    bring_ffn = [
+        [
+            bring(
+                6 + 2 * (block % 4) + part,
+                ref.at[:, pl.ds(block * LANES, LANES)],
+                w_ffn.at[own_rows(shard), pl.ds(block * pair_width + part * LANES, LANES)],
             )
-        bring_ffn.append(pair)
+            for part, ref in enumerate((ffn_gate_ref, ffn_up_ref))
+        ]
+        for block in range(ffn_blocks)
+    ]
     bring_down = [
-        bring(ffn_down_ref.at[:, pl.ds(c * LANES, LANES)], w_down.at[c, :, own_rows(LANES)])
+        bring(14 + c, ffn_down_ref.at[:, pl.ds(c * LANES, LANES)], w_down.at[c, :, own_rows(LANES)])
         for c in range(down_chunks)
     ]
 
@@ -248,18 +246,30 @@
     for block in range(ffn_blocks):
         chunks.append((row_chunk(w_ffn, block * pair_width), bring_ffn[block]))
 
-    def down_view(c):
+    def down_view(c, first, size):
         def view(s, half):
-            size = w_down.shape[1] // 2
-            return w_down.at[c, own_rows(size, half), own_rows(LANES, s)]
+            rows_here = pl.ds(pl.multiple_of(first + half * (size // 2), LANES // 2), size // 2)
+            return w_down.at[c, rows_here, own_rows(LANES, s)]
 
         return view
 
-    for c in range(down_chunks):
-        chunks.append((down_view(c), [bring_down[c]]))
+    hidden_width = w_down.shape[1]
+    split = (ffn_blocks + 1) // 2 * LANES
+    for c in range(down_chunks - 1):
+        chunks.append((down_view(c, 0, hidden_width), [bring_down[c]]))
+    chunks.append((down_view(down_chunks - 1, 0, split), [bring_down[-1]]))
+    chunks.append((down_view(down_chunks - 1, split, hidden_width - split), []))
     total = len(chunks)
     first_ffn = mix_chunks + 1
+    out_at_step = mix_chunks + 3
     first_down = first_ffn + ffn_blocks
+    first_copies = 5
+
+    for k in range(first_copies):
+        if k == 1:
+            bring_tokens.start()
+        for copy in chunks[k][1]:
+            copy.start()
 
     barrier = pltpu.get_barrier_semaphore()
     for target in (
@@ -268,36 +278,50 @@
         pl.semaphore_signal(barrier, inc=1, device_id=target, device_id_type=MESH)
     pl.semaphore_wait(barrier, 5)
 
-    def z_copy(k, d, hop, s, target):
+    def place(d, hop, receiver):
+        return hop - 1 if d == 0 else receiver + hop - 1
+
+    def z_copy(k, d, hop, s, target, receiver):
         view = chunks[k][0](s, rep)
         return pltpu.make_async_remote_copy(
-            src_ref=view, dst_ref=view, send_sem=z_send.at[k, d, hop - 1], recv_sem=z_recv.at[k, d, hop - 1],
-            device_id={"fs": target}, device_id_type=MESH,
+            src_ref=view, dst_ref=view, send_sem=z_send.at[k % 3, d, hop - 1],
+            recv_sem=z_recv.at[k, place(d, hop, receiver)], device_id={"fs": target}, device_id_type=MESH,
+        )
+
+    def extra_copy(k, d, target):
+        view = chunks[k][0](here, 1 - rep)
+        return pltpu.make_async_remote_copy(
+            src_ref=view, dst_ref=view, send_sem=z_send.at[k % 3, d, 3],
+            recv_sem=x_recv.at[k, place(d, 1, target)], device_id={"fs": target}, device_id_type=MESH,
         )
 
     def x_copy(k, d, hop, s, half):
         view = chunks[k][0](s, half)
         return pltpu.make_async_remote_copy(
-            src_ref=view, dst_ref=view, send_sem=x_send.at[k, d, hop - 1], recv_sem=x_recv.at[k, d, hop - 1],
-            device_id={"rep": 1 - rep}, device_id_type=MESH,
+            src_ref=view, dst_ref=view, send_sem=x_send.at[k % 3, d, hop - 1],
+            recv_sem=x_recv.at[k, place(d, hop, here)], device_id={"rep": 1 - rep}, device_id_type=MESH,
         )
 
     pending = {}
+    late = []
+    at_end = jnp.logical_or(here == 0, here == 3)
+
+    def guarded(step, guard, make):
+        @pl.when(guard)
+        def _():
+            make().start()
+
+        def finish():
+            @pl.when(guard)
+            def _():
+                make().wait_send()
+
+        pending.setdefault(step, []).append(finish)
 
     def z_send_start(step, k, d, hop, guard):
         s = here - (hop - 1) if d == 0 else here + (hop - 1)
         target = here + 1 if d == 0 else here - 1
-
-        @pl.when(guard)
-        def _():
-            z_copy(k, d, hop, s, target).start()
-
-        def finish():
-            @pl.when(guard)
-            def _():
-                z_copy(k, d, hop, s, target).wait_send()
-
-        pending.setdefault(step, []).append(finish)
+        guarded(step, guard, lambda: z_copy(k, d, hop, s, target, target))
 
     def own_send(step, k):
         for copy in chunks[k][1]:
@@ -305,6 +329,10 @@
         z_send_start(step, k, 0, 1, here <= 2)
         z_send_start(step, k, 1, 1, here >= 1)
 
+    def extra_send(step, k):
+        guarded(step, here <= 1, lambda: extra_copy(k, 0, here + 1))
+        guarded(step, here >= 2, lambda: extra_copy(k, 1, here - 1))
+
     def arrive(step, k, d, hop):
         s = here - hop if d == 0 else here + hop
         origin = here - 1 if d == 0 else here + 1
@@ -312,22 +340,17 @@
 
         @pl.when(valid)
         def _():
-            z_copy(k, d, hop, s, origin).wait_recv()
+            z_copy(k, d, hop, s, origin, here).wait_recv()
 
         if hop < 3:
             onward = here <= 2 if d == 0 else here >= 1
             z_send_start(step, k, d, hop + 1, jnp.logical_and(valid, onward))
-
-        @pl.when(valid)
-        def _():
-            x_copy(k, d, hop, s, rep).start()
-
-        def finish():
-            @pl.when(valid)
-            def _():
-                x_copy(k, d, hop, s, rep).wait_send()
-
-        pending.setdefault(step, []).append(finish)
+        crosses = jnp.logical_and(valid, at_end) if hop == 1 else valid
+        cross = lambda: guarded(step, crosses, lambda: x_copy(k, d, hop, s, rep))
+        if k == total - 1 and hop < 3:
+            late.append(cross)
+        else:
+            cross()
 
     def x_arrive(k, d, hop):
         s = here - hop if d == 0 else here + hop
@@ -341,22 +364,31 @@
         for finish in pending.pop(step, ()):
             finish()
 
-    def advance(step):
-        finish_sends(step - 2)
-        if step == 0:
-            own_send(0, 0)
-        if step + 1 < total:
-            own_send(step, step + 1)
-        for hop in (1, 2, 3):
-            k = step - hop + 1
-            if 0 <= k < total:
+    def sent_at(k):
+        return max(0, k - 1 if k <= out_at_step else k - 2)
+
+    def advance(step, hop):
+        if hop == 1:
+            finish_sends(step - 2)
+            for k in range(total):
+                if sent_at(k) == step:
+                    own_send(step, k)
+            if step + first_copies < total:
+                for copy in chunks[step + first_copies][1]:
+                    copy.start()
+        k = step - hop + 1
+        if 0 <= k < total:
+            for d in (0, 1):
+                arrive(step, k, d, hop)
+        if hop == 1 and 0 <= step - 1 < total:
+            extra_send(step, step - 1)
+        if hop == 3:
+            while late:
+                late.pop(0)()
+        if hop == 3 and 0 <= step - 3 < total:
+            for leg in (1, 2, 3):
                 for d in (0, 1):
-                    arrive(step, k, d, hop)
-        for hop in (1, 2, 3):
-            k = step - hop
-            if 0 <= k < total:
-                for d in (0, 1):
-                    x_arrive(k, d, hop)
+                    x_arrive(step - 3, d, leg)
 
     y_index = {}
     for name in ("gather1", "gather2", "reduce1"):
@@ -365,11 +397,15 @@
     for leg in ("beside", "across", "corner"):
         y_index["reduce2", leg] = 9 * seqs + (len(y_index) - 9) * seqs * down_chunks
 
-    def y_copy(name, leg, index, source, target, to):
-        slot = y_index[name, leg] + index
+    send_group = {"gather1": 0, "gather2": 0, "reduce1": 1, "reduce2": 2}
+    legs = ("beside", "across", "corner")
+
+    def y_copy(name, leg, index, source, target, to, send_index=None):
+        group = send_group[name] * 3 * seqs + legs.index(leg) * (2 * seqs if name == "reduce2" else seqs)
         return pltpu.make_async_remote_copy(
-            src_ref=source, dst_ref=target, send_sem=y_send.at[slot], recv_sem=y_recv.at[slot],
-            device_id={"tp": to}, device_id_type=MESH,
+            src_ref=source, dst_ref=target,
+            send_sem=y_send.at[group + (index if send_index is None else send_index)],
+            recv_sem=y_recv.at[y_index[name, leg] + index], device_id={"tp": to}, device_id_type=MESH,
         )
 
     def seq_rows(j):
@@ -399,7 +435,7 @@
     def norm_into(source, gain_ref, target, source_row, target_row):
         group = 16
 
-        @pl.loop(0, SEQ // group)
+        @pl.loop(0, SEQ // group, unroll=4)
         def _(i):
             offset = pl.multiple_of(i * group, group)
             floats = source[pl.ds(source_row + offset, group), :].astype(f32)
@@ -413,11 +449,13 @@
             rate = rate_ref[pl.ds(tp * heads + head, 1), :]
             mask[head] = jnp.where(gap >= 0, jnp.exp(positive * rate), 0.0)
 
-    def mix(j):
+    def project(j):
         gather_wait("gather1", x_all, "beside", j)
         gather_wait("gather1", x_all, "corner", j)
         norm_into(x_all, mix_gain_ref, normed, j * SEQ, 0)
         proj[...] = jnp.dot(normed[...], w_mix[...], preferred_element_type=f32).astype(bf16)
+
+    def retain():
         highest = lax.Precision.HIGHEST
         lane = lax.broadcasted_iota(jnp.int32, (SEQ, key_width), 1)
         cosine, sine = cos_ref[...], sin_ref[...]
@@ -445,8 +483,9 @@
             gate = proj[:, first : first + DV].astype(f32)
             mixed[:, head * DV : (head + 1) * DV] = (grouped * jax.nn.silu(gate)).astype(bf16)
 
-    def reduce_copy(name, leg, index, source, target):
-        return y_copy(name, leg, index, source, target, across_id if leg == "across" else beside_id)
+    def reduce_copy(name, leg, index, source, target, send_index=None):
+        to = across_id if leg == "across" else beside_id
+        return y_copy(name, leg, index, source, target, to, send_index)
 
     def mix_reduce(j):
         def quarter(owner):
@@ -482,41 +521,70 @@
         gather_wait("gather2", res_all, "corner", j)
         norm_into(res_all, ffn_gain_ref, normed_ffn, j * SEQ, j * SEQ)
 
-    def ffn(first, last):
-        @pl.loop(first, last)
-        def _(b):
-            weight_columns = own_rows(pair_width, b)
-            hidden_columns = own_rows(LANES, b)
-
-            @pl.loop(0, seqs)
-            def _(j):
-                part = own_rows(SEQ, j)
-                both = jnp.dot(normed_ffn[part, :], w_ffn[:, weight_columns], preferred_element_type=f32)
-                hidden[part, hidden_columns] = (jax.nn.silu(both[:, :LANES]) * both[:, LANES:]).astype(bf16)
+    def ffn(b):
+        group = FFN_ROWS * SEQ
+        weight = w_ffn.at[:, pl.ds(b * pair_width, pair_width)]
+
+        @pl.loop(0, rows // group)
+        def _(j):
+            part = own_rows(group, j)
+            both = jnp.dot(normed_ffn[part, :], weight[...], preferred_element_type=f32)
+            hidden[part, b * LANES : (b + 1) * LANES] = (
+                jax.nn.silu(both[:, :LANES]) * both[:, LANES:]
+            ).astype(bf16)
 
     def reduce2(leg, c, j, source, target):
         part = own_rows(SEQ, j)
-        return reduce_copy("reduce2", leg, c * seqs + j, source.at[c, part, :], target.at[c, part, :])
+        slot = (c % 2) * seqs + j
+        return reduce_copy("reduce2", leg, c * seqs + j, source.at[c, part, :], target.at[c, part, :], slot)
+
+    def down_products(c, j):
+        part = own_rows(SEQ, j)
+        if c + 1 < down_chunks:
+            sums[...] = jnp.dot(hidden[part, :], w_down[c], preferred_element_type=f32)
+        else:
+            sums[...] = begun[part, :] + jnp.dot(
+                hidden[part, split:], w_down[c, split:, :], preferred_element_type=f32
+            )
+        corner2[c, part, :] = sums[:, own_rows(LANES, corner_id)].astype(bf16)
+        reduce2("corner", c, j, corner2, corner2_in).start()
+        beside2[c, part, :] = sums[:, own_rows(LANES, beside_id)].astype(bf16)
+        reduce2("beside", c, j, beside2, beside2_in).start()
+        far2[part, :] = sums[:, own_rows(LANES, across_id)]
+        own2[c, part, :] = sums[:, own_rows(LANES, tp)]
+
+    def down_begin(c):
+        @pl.loop(0, seqs)
+        def _(j):
+            part = own_rows(SEQ, j)
+            begun[part, :] = jnp.dot(hidden[part, :split], w_down[c, :split, :], preferred_element_type=f32)
+
+    def down_onward(c, j):
+        part = own_rows(SEQ, j)
+        reduce2("corner", c, j, corner2, corner2_in).wait_recv()
+        across2[c, part, :] = (far2[part, :] + corner2_in[c, part, :].astype(f32)).astype(bf16)
+        reduce2("across", c, j, across2, across2_in).start()
 
     def down(c):
         @pl.loop(0, seqs)
         def _(j):
-            part = own_rows(SEQ, j)
-            left = hidden[part, :]
-            far = jnp.dot(left, w_down[c, :, own_rows(pair_width, 1 - chip)], preferred_element_type=f32)
-            lower, upper = far[:, :LANES], far[:, LANES:]
-            corner2[c, part, :] = jnp.where(core == 0, upper, lower).astype(bf16)
-            sent = reduce2("corner", c, j, corner2, corner2_in)
-            sent.start()
-            onward = jnp.where(core == 0, lower, upper)
-            near = jnp.dot(left, w_down[c, :, own_rows(pair_width, chip)], preferred_element_type=f32)
-            lower, upper = near[:, :LANES], near[:, LANES:]
-            beside2[c, part, :] = jnp.where(core == 0, upper, lower).astype(bf16)
-            reduce2("beside", c, j, beside2, beside2_in).start()
-            own2[c, part, :] = jnp.where(core == 0, lower, upper)
-            sent.wait_recv()
-            across2[c, part, :] = (onward + corner2_in[c, part, :].astype(f32)).astype(bf16)
-            reduce2("across", c, j, across2, across2_in).start()
+            down_products(c, j)
+
+    def down_rest(c):
+        @pl.loop(0, seqs)
+        def _(j):
+            down_onward(c, j)
+
+    def down_last(c):
+        @pl.loop(0, seqs + 1)
+        def _(j):
+            @pl.when(j < seqs)
+            def _():
+                down_products(c, j)
+
+            @pl.when(j > 0)
+            def _():
+                down_onward(c, j - 1)
 
     def finish_down(c):
         @pl.loop(0, seqs)
@@ -527,61 +595,73 @@
             share = own2[c, part, :] + beside2_in[c, part, :].astype(f32) + across2_in[c, part, :].astype(f32)
             columns = pl.ds(pl.multiple_of(tp * width + c * LANES, LANES), LANES)
             kept = res_all[part, columns].astype(f32)
-            out_ref[part, c * LANES : (c + 1) * LANES] = (kept + share).astype(bf16)
+            result[c, part, :] = (kept + share).astype(bf16)
             for leg, source, target in (
                 ("corner", corner2, corner2_in), ("beside", beside2, beside2_in), ("across", across2, across2_in),
             ):
                 reduce2(leg, c, j, source, target).wait_send()
 
+        out_copy(c).start()
+
+    def out_copy(c):
+        return pltpu.make_async_copy(result.at[c], out_ref.at[:, pl.ds(c * LANES, LANES)], out_sem.at[c])
+
     work = {}
 
-    def at(step, function, *args):
-        work.setdefault(step, []).append((function, args))
+    def at(slot, function, *args):
+        work.setdefault(slot, []).append((function, args))
 
     at(0, make_mask)
     for j in range(seqs):
-        at(1 + j, relay, "gather1", x_all, j)
-    mixed_at = mix_chunks + 2
-    out_at = mixed_at + 1
-    order = []
-    for j in range(seqs):
-        at(out_at + j + 3, ready, j)
-    for j in range(seqs):
-        at(out_at + j + 2, relay, "gather2", res_all, j)
-    for j in range(seqs):
-        at(out_at + j + 1, residual, j)
-    for j in range(seqs):
-        at(out_at + j, mix_reduce, j)
-    for j in range(seqs):
-        at(mixed_at + j, mix, j)
-    done = 0
-    ffn_from = out_at + seqs + 2
-    for step in range(ffn_from, first_down + 3):
-        there = min(ffn_blocks, step - first_ffn - 2)
-        last = min(there, done + 4)
-        if step == first_down + 2:
-            last = ffn_blocks
-        if last > done:
-            at(step, ffn, done, last)
-            done = last
-    for c in range(down_chunks):
-        at(first_down + 3 + c, down, c)
-        if c:
-            at(first_down + 3 + c, finish_down, c - 1)
+        at(5 + 3 * j, relay, "gather1", x_all, j)
+    base = 3 * (mix_chunks + 2) + 2
+    for j, (a, b, r, s, l, n) in enumerate(PLAN):
+        at(base + s, residual, j)
+        at(base + l, relay, "gather2", res_all, j)
+        at(base + n, ready, j)
+        at(base + b, retain)
+        at(base + r, mix_reduce, j)
+        at(base + a, project, j)
+    def finish_gather():
+        for copy in y_pending[: 3 * seqs]:
+            copy.wait_send()
+        del y_pending[: 3 * seqs]
+
+    at(base + min(r for _, _, r, *_ in PLAN), finish_gather)
+    slot = base + 1 + max(n for *_, n in PLAN)
+    for block in range(ffn_blocks):
+        slot = max(slot, 3 * (first_ffn + block + 3) + 2)
+        at(slot, ffn, block)
+        slot += 1 if slot % 3 != FFN_PER_STEP - 1 else 4 - FFN_PER_STEP
+    for c in range(down_chunks - 1):
+        complete = 3 * (first_down + 3 + c) + 2
+        if c + 2 < down_chunks:
+            at(complete, down, c)
+            at(complete + 1, down_rest, c)
+        else:
+            at(complete, down_last, c)
+        if c + 2 < down_chunks:
+            at(complete + 5, finish_down, c)
+    last_slot = 3 * (total + 3) - 1
+    at(last_slot - 3, down_begin, down_chunks - 1)
 
     bring_tokens.wait()
     for j in range(seqs):
         gather_send("gather1", x_all, "across", j)
         gather_send("gather1", x_all, "beside", j)
-    for step in range(total + 3):
-        advance(step)
-        for function, args in work.get(step, ()):
+    for slot in range(3 * (total + 3)):
+        advance(slot // 3, slot % 3 + 1)
+        for function, args in work.get(slot, ()):
             function(*args)
+    down_last(down_chunks - 1)
+    finish_down(down_chunks - 2)
     finish_down(down_chunks - 1)
     for step in sorted(pending):
         finish_sends(step)
     for copy in y_pending:
         copy.wait_send()
+    for c in range(down_chunks):
+        out_copy(c).wait()
 
 
 def layer(
@@ -597,7 +677,7 @@
     mix_width = 2 * key_width + 2 * value_width
     hidden_width = ffn_gate.shape[1]
     blocks, down_chunks = hidden_width // LANES, ffn_down.shape[1] // LANES
-    total = mix_width // (2 * LANES) + 1 + blocks + down_chunks
+    total = mix_width // (2 * LANES) + 1 + blocks + down_chunks + 1
     frequency = rope_base ** (-np.linspace(0.0, 1.0, DK // 2))
     angles = np.arange(SEQ)[:, None] * frequency[None, :]
     cosine = np.tile(np.repeat(np.cos(angles), 2, axis=1), (1, heads)).astype(np.float32)
@@ -612,7 +692,7 @@
         fused_kernel,
         out_shape=jax.ShapeDtypeStruct((rows, width), bf16),
         in_specs=[anywhere, vmem] + [anywhere] * 5 + [vmem, vmem] + [anywhere] * 3 + [vmem] * 3,
-        out_specs=vmem,
+        out_specs=anywhere,
         scratch_shapes=[
             pltpu.VMEM((model, mix_width), bf16),
             pltpu.VMEM((out_weight.shape[0], model), bf16),
@@ -630,15 +710,22 @@
         + first_sum
         + [pltpu.VMEM((seqs, SEQ, width), f32)]
         + second_sum
-        + [pltpu.VMEM((down_chunks, rows, LANES), f32)]
         + [
-            dma((6 + 2 * blocks + down_chunks,)),
-            dma((total, 2, 3)),
-            dma((total, 2, 3)),
-            dma((total, 2, 3)),
-            dma((total, 2, 3)),
+            pltpu.VMEM((down_chunks, rows, LANES), f32),
+            pltpu.VMEM((rows, LANES), f32),
+            pltpu.VMEM((SEQ, 4 * LANES), f32),
+            pltpu.VMEM((rows, 4 * LANES), f32),
+            pltpu.VMEM((down_chunks, rows, LANES), bf16),
+        ]
+        + [
+            dma((14 + down_chunks,)),
+            dma((3, 2, 4)),
+            dma((total, 3)),
+            dma((3, 2, 3)),
+            dma((total, 3)),
+            dma((12 * seqs,)),
             dma((9 * seqs + 3 * seqs * down_chunks,)),
-            dma((9 * seqs + 3 * seqs * down_chunks,)),
+            dma((down_chunks,)),
         ],
         compiler_params=pltpu.CompilerParams(
             collective_id=0, has_side_effects=True, vmem_limit_bytes=67043328

time: 227 us -> 206 us (0.907)
  Pallas kernels: 224 us -> 204 us
    pallas_call x1, Pallas kernels: 224 us -> 204 us  [layer(): pl.pallas_call(fused_kernel, out_shape=jax.ShapeDtypeStruct((rows, width)...]
where the time goes in v1:
time: 206 us
  Pallas kernels  204 us (99%)
  local copies, waits for them, and re-layouts  2.26 us (1%)
    pallas_call x1, Pallas kernels, layer(): pl.pallas_call(fused_kernel, out_shape=jax.ShapeDtypeStruct((rows, width)...  204 us

profile of v1, /device:TPU:0, one launch (start us, length us, event | category | flops | bytes accessed | tf_op | source)
XLA Modules:
  0.0 206.0 jit_solution(2729003882026945678)
XLA Ops:
  0.0 203.7 %layer.1 = bf16[1024,512]{1,0:T(8,128)(2,1)} custom-call(bf16[1024,512]{1,0:T(8,128)(2,1)} %tokens_ref.1, f32[1,2048]{1,0:T(1,128)} %bitcast.2, bf16[512,128]{1,0:T(8,128)(2,1)} %query_ref.1, bf16[512,128]{1,0:T(8,128)(2,1)} %key_ref.1, bf16[512,256]{1,0:T(8,128)(2,1)} %value_ref.1, bf16[512,256]{1,0:T(8,128)(2,1)} %gate_ref.1, ...), custom_call_target="tpu_custom_call" | custom-call | tf_op jit(solution)/shard_map/layer/pallas_call | solution.py:691
  203.7 2.3 %copy.17 = bf16[1024,512]{1,0:T(8,128)(2,1)} copy(bf16[1024,512]{1,0:T(8,128)(2,1)} %layer.1) | data formatting | bytes 2097152

commit v2 on v1

--- a/solution.py
+++ b/solution.py
@@ -167,13 +167,14 @@
 LANES = 128
 FFN_ROWS = 2
 FFN_PER_STEP = 3
-PLAN = ((0, 1, 3, 6, 10, 12), (2, 4, 5, 8, 14, 16), (5, 6, 7, 12, 18, 19), (8, 9, 11, 16, 20, 21))
+PLAN = ((0, 1, 3, 6, 10, 12), (2, 4, 5, 8, 14, 16), (5, 6, 7, 12, 19, 20), (8, 9, 11, 17, 21, 22))
 
 
 def fused_kernel(
-    tokens_ref, mix_gain_ref, query_ref, key_ref, value_ref, gate_ref, proj_out_ref, head_gain_ref,
-    ffn_gain_ref, ffn_gate_ref, ffn_up_ref, ffn_down_ref, cos_ref, sin_ref, rate_ref,
+    tokens_ref, mix_gain_hbm, query_ref, key_ref, value_ref, gate_ref, proj_out_ref, head_gain_hbm,
+    ffn_gain_hbm, ffn_gate_ref, ffn_up_ref, ffn_down_ref, cos_hbm, sin_hbm, rate_hbm,
     out_ref,
+    mix_gain_ref, head_gain_ref, ffn_gain_ref, cos_ref, sin_ref, rate_ref,
     w_mix, w_out, w_ffn, w_down, x_all, res_all, normed, normed_ffn, proj, mixed, hidden, mask,
     corner1, corner1_in, beside1, beside1_in, across1, across1_in, own1,
     corner2, corner2_in, beside2, beside2_in, across2, across2_in, own2, far2, sums, begun, result,
@@ -195,6 +196,12 @@
     def own_rows(size, base=None):
         index = here if base is None else base
         return pl.ds(pl.multiple_of(index * size, size), size)
+
+    barrier = pltpu.get_barrier_semaphore()
+    for target in (
+        {"fs": (here + 1) % 4}, {"fs": (here + 3) % 4}, {"rep": 1 - rep}, {"tp": beside_id}, {"tp": across_id},
+    ):
+        pl.semaphore_signal(barrier, inc=1, device_id=target, device_id_type=MESH)
 
     def bring(slot, source, target):
         return pltpu.make_async_copy(source, target, local_sem.at[slot])
@@ -261,7 +268,6 @@
     chunks.append((down_view(down_chunks - 1, split, hidden_width - split), []))
     total = len(chunks)
     first_ffn = mix_chunks + 1
-    out_at_step = mix_chunks + 3
     first_down = first_ffn + ffn_blocks
     first_copies = 5
 
@@ -270,12 +276,17 @@
             bring_tokens.start()
         for copy in chunks[k][1]:
             copy.start()
-
-    barrier = pltpu.get_barrier_semaphore()
-    for target in (
-        {"fs": (here + 1) % 4}, {"fs": (here + 3) % 4}, {"rep": 1 - rep}, {"tp": beside_id}, {"tp": across_id},
-    ):
-        pl.semaphore_signal(barrier, inc=1, device_id=target, device_id_type=MESH)
+    bring_small = [
+        bring(14 + down_chunks + i, source, target)
+        for i, (source, target) in enumerate(
+            (
+                (mix_gain_hbm, mix_gain_ref), (head_gain_hbm, head_gain_ref), (ffn_gain_hbm, ffn_gain_ref),
+                (cos_hbm, cos_ref), (sin_hbm, sin_ref), (rate_hbm, rate_ref),
+            )
+        )
+    ]
+    for copy in bring_small:
+        copy.start()
     pl.semaphore_wait(barrier, 5)
 
     def place(d, hop, receiver):
@@ -365,14 +376,17 @@
             finish()
 
     def sent_at(k):
-        return max(0, k - 1 if k <= out_at_step else k - 2)
+        return max(0, k - 1)
 
     def advance(step, hop):
         if hop == 1:
-            finish_sends(step - 2)
+            if step <= total:
+                finish_sends(step - 2)
             for k in range(total):
                 if sent_at(k) == step:
                     own_send(step, k)
+                    if k == 0:
+                        send_tokens()
             if step + first_copies < total:
                 for copy in chunks[step + first_copies][1]:
                     copy.start()
@@ -443,6 +457,8 @@
             target[pl.ds(target_row + offset, group), :] = (floats * scale * gain_ref[...]).astype(bf16)
 
     def make_mask():
+        for copy in bring_small:
+            copy.wait()
         gap = lax.broadcasted_iota(jnp.int32, (SEQ, SEQ), 0) - lax.broadcasted_iota(jnp.int32, (SEQ, SEQ), 1)
         positive = jnp.maximum(gap, 0).astype(f32)
         for head in range(heads):
@@ -645,10 +661,12 @@
     last_slot = 3 * (total + 3) - 1
     at(last_slot - 3, down_begin, down_chunks - 1)
 
-    bring_tokens.wait()
-    for j in range(seqs):
-        gather_send("gather1", x_all, "across", j)
-        gather_send("gather1", x_all, "beside", j)
+    def send_tokens():
+        bring_tokens.wait()
+        for j in range(seqs):
+            gather_send("gather1", x_all, "across", j)
+            gather_send("gather1", x_all, "beside", j)
+
     for slot in range(3 * (total + 3)):
         advance(slot // 3, slot % 3 + 1)
         for function, args in work.get(slot, ()):
@@ -684,16 +702,22 @@
     sine = np.tile(np.repeat(np.sin(angles), 2, axis=1), (1, heads)).astype(np.float32)
     rates = np.log1p(-np.exp2(-5.0 - 4.0 * np.arange(HEADS) / (HEADS - 1)))
     rates = np.broadcast_to(rates[:, None], (HEADS, SEQ)).astype(np.float32)
-    vmem, anywhere = pl.BlockSpec(memory_space=pltpu.VMEM), pl.BlockSpec(memory_space=pl.ANY)
+    anywhere = pl.BlockSpec(memory_space=pl.ANY)
     first_sum = [pltpu.VMEM((seqs, SEQ, width), bf16)] * 6
     second_sum = [pltpu.VMEM((down_chunks, rows, LANES), bf16)] * 6
     dma = pltpu.SemaphoreType.DMA
     return pl.pallas_call(
         fused_kernel,
         out_shape=jax.ShapeDtypeStruct((rows, width), bf16),
-        in_specs=[anywhere, vmem] + [anywhere] * 5 + [vmem, vmem] + [anywhere] * 3 + [vmem] * 3,
+        in_specs=[anywhere] * 15,
         out_specs=anywhere,
         scratch_shapes=[
+            pltpu.VMEM((1, model), f32),
+            pltpu.VMEM(head_gain.shape, f32),
+            pltpu.VMEM((1, model), f32),
+            pltpu.VMEM(cosine.shape, f32),
+            pltpu.VMEM(sine.shape, f32),
+            pltpu.VMEM(rates.shape, f32),
             pltpu.VMEM((model, mix_width), bf16),
             pltpu.VMEM((out_weight.shape[0], model), bf16),
             pltpu.VMEM((model, 2 * hidden_width), bf16),
@@ -718,7 +742,7 @@
             pltpu.VMEM((down_chunks, rows, LANES), bf16),
         ]
         + [
-            dma((14 + down_chunks,)),
+            dma((20 + down_chunks,)),
             dma((3, 2, 4)),
             dma((total, 3)),
             dma((3, 2, 3)),

time: 206 us -> 203 us (0.985)
  Pallas kernels: 204 us -> 200 us
    pallas_call x1, Pallas kernels: 204 us -> 200 us  [layer(): pl.pallas_call(fused_kernel, out_shape=jax.ShapeDtypeStruct((rows, width)...]
where the time goes in v2:
time: 203 us; the launch traced here: 202 us
  Pallas kernels  200 us (99%)
  local copies, waits for them, and re-layouts  2.26 us (1%)
    pallas_call x1, Pallas kernels, layer(): pl.pallas_call(fused_kernel, out_shape=jax.ShapeDtypeStruct((rows, width)...  200 us

profile of v2, /device:TPU:0, one launch (start us, length us, event | category | flops | bytes accessed | tf_op | source)
XLA Modules:
  0.0 202.5 jit_solution(14832338326646570604)
XLA Ops:
  0.0 200.2 %layer.1 = bf16[1024,512]{1,0:T(8,128)(2,1)} custom-call(bf16[1024,512]{1,0:T(8,128)(2,1)} %tokens_ref.1, f32[1,2048]{1,0:T(1,128)} %bitcast.2, bf16[512,128]{1,0:T(8,128)(2,1)} %query_ref.1, bf16[512,128]{1,0:T(8,128)(2,1)} %key_ref.1, bf16[512,256]{1,0:T(8,128)(2,1)} %value_ref.1, bf16[512,256]{1,0:T(8,128)(2,1)} %gate_ref.1, ...), custom_call_target="tpu_custom_call" | custom-call | tf_op jit(solution)/shard_map/layer/pallas_call | solution.py:709
  200.2 2.3 %copy.17 = bf16[1024,512]{1,0:T(8,128)(2,1)} copy(bf16[1024,512]{1,0:T(8,128)(2,1)} %layer.1) | data formatting | bytes 2097152

commit v3 on v2

--- a/solution.py
+++ b/solution.py
@@ -166,7 +166,8 @@
 MESH = pl.DeviceIdType.MESH
 LANES = 128
 FFN_ROWS = 2
-FFN_PER_STEP = 3
+FFN_BLOCKS = 1
+FFN_STRIDE = 1
 PLAN = ((0, 1, 3, 6, 10, 12), (2, 4, 5, 8, 14, 16), (5, 6, 7, 12, 19, 20), (8, 9, 11, 17, 21, 22))
 
 
@@ -177,7 +178,7 @@
     mix_gain_ref, head_gain_ref, ffn_gain_ref, cos_ref, sin_ref, rate_ref,
     w_mix, w_out, w_ffn, w_down, x_all, res_all, normed, normed_ffn, proj, mixed, hidden, mask,
     corner1, corner1_in, beside1, beside1_in, across1, across1_in, own1,
-    corner2, corner2_in, beside2, beside2_in, across2, across2_in, own2, far2, sums, begun, result,
+    corner2, corner2_in, beside2, beside2_in, across2, across2_in, own2, far2, sums, result,
     local_sem, z_send, z_recv, x_send, x_recv, y_send, y_recv, out_sem,
 ):
     f32, bf16 = jnp.float32, jnp.bfloat16
@@ -253,20 +254,26 @@
     for block in range(ffn_blocks):
         chunks.append((row_chunk(w_ffn, block * pair_width), bring_ffn[block]))
 
-    def down_view(c, first, size):
+    def down_view(c):
         def view(s, half):
-            rows_here = pl.ds(pl.multiple_of(first + half * (size // 2), LANES // 2), size // 2)
-            return w_down.at[c, rows_here, own_rows(LANES, s)]
+            return w_down.at[c, own_rows(w_down.shape[1] // 2, half), own_rows(LANES, s)]
 
         return view
 
-    hidden_width = w_down.shape[1]
-    split = (ffn_blocks + 1) // 2 * LANES
-    for c in range(down_chunks - 1):
-        chunks.append((down_view(c, 0, hidden_width), [bring_down[c]]))
-    chunks.append((down_view(down_chunks - 1, 0, split), [bring_down[-1]]))
-    chunks.append((down_view(down_chunks - 1, split, hidden_width - split), []))
+    for c in range(down_chunks):
+        chunks.append((down_view(c), [bring_down[c]]))
+    chunks.append((down_view(down_chunks - 1), []))
     total = len(chunks)
+
+    def travels(k, s):
+        if k < total - 2:
+            return True
+        other_chip = jnp.logical_xor(s >= 2, chip == 1)
+        return other_chip if k == total - 2 else jnp.logical_not(other_chip)
+
+    def allowed(guard, k, s):
+        return guard if k < total - 2 else jnp.logical_and(guard, travels(k, s))
+
     first_ffn = mix_chunks + 1
     first_down = first_ffn + ffn_blocks
     first_copies = 5
@@ -315,7 +322,6 @@
 
     pending = {}
     late = []
-    at_end = jnp.logical_or(here == 0, here == 3)
 
     def guarded(step, guard, make):
         @pl.when(guard)
@@ -332,7 +338,7 @@
     def z_send_start(step, k, d, hop, guard):
         s = here - (hop - 1) if d == 0 else here + (hop - 1)
         target = here + 1 if d == 0 else here - 1
-        guarded(step, guard, lambda: z_copy(k, d, hop, s, target, target))
+        guarded(step, allowed(guard, k, s), lambda: z_copy(k, d, hop, s, target, target))
 
     def own_send(step, k):
         for copy in chunks[k][1]:
@@ -341,13 +347,13 @@
         z_send_start(step, k, 1, 1, here >= 1)
 
     def extra_send(step, k):
-        guarded(step, here <= 1, lambda: extra_copy(k, 0, here + 1))
-        guarded(step, here >= 2, lambda: extra_copy(k, 1, here - 1))
+        guarded(step, allowed(here == 0, k, here), lambda: extra_copy(k, 0, here + 1))
+        guarded(step, allowed(here == 3, k, here), lambda: extra_copy(k, 1, here - 1))
 
     def arrive(step, k, d, hop):
         s = here - hop if d == 0 else here + hop
         origin = here - 1 if d == 0 else here + 1
-        valid = here >= hop if d == 0 else here + hop <= 3
+        valid = allowed(here >= hop if d == 0 else here + hop <= 3, k, s)
 
         @pl.when(valid)
         def _():
@@ -356,7 +362,7 @@
         if hop < 3:
             onward = here <= 2 if d == 0 else here >= 1
             z_send_start(step, k, d, hop + 1, jnp.logical_and(valid, onward))
-        crosses = jnp.logical_and(valid, at_end) if hop == 1 else valid
+        crosses = jnp.logical_and(valid, here != 1 + d) if hop == 1 else valid
         cross = lambda: guarded(step, crosses, lambda: x_copy(k, d, hop, s, rep))
         if k == total - 1 and hop < 3:
             late.append(cross)
@@ -365,7 +371,7 @@
 
     def x_arrive(k, d, hop):
         s = here - hop if d == 0 else here + hop
-        valid = here >= hop if d == 0 else here + hop <= 3
+        valid = allowed(here >= hop if d == 0 else here + hop <= 3, k, s)
 
         @pl.when(valid)
         def _():
@@ -374,6 +380,9 @@
     def finish_sends(step):
         for finish in pending.pop(step, ()):
             finish()
+
+    def complete_at(k):
+        return 3 * (k + 3) + 2
 
     def sent_at(k):
         return max(0, k - 1)
@@ -397,12 +406,13 @@
         if hop == 1 and 0 <= step - 1 < total:
             extra_send(step, step - 1)
         if hop == 3:
-            while late:
+            while late and step >= total:
                 late.pop(0)()
-        if hop == 3 and 0 <= step - 3 < total:
-            for leg in (1, 2, 3):
-                for d in (0, 1):
-                    x_arrive(step - 3, d, leg)
+        for k in range(total):
+            if complete_at(k) == 3 * step + hop - 1:
+                for leg in (1, 2, 3):
+                    for d in (0, 1):
+                        x_arrive(k, d, leg)
 
     y_index = {}
     for name in ("gather1", "gather2", "reduce1"):
@@ -415,7 +425,7 @@
     legs = ("beside", "across", "corner")
 
     def y_copy(name, leg, index, source, target, to, send_index=None):
-        group = send_group[name] * 3 * seqs + legs.index(leg) * (2 * seqs if name == "reduce2" else seqs)
+        group = send_group[name] * 3 * seqs + legs.index(leg) * (3 * seqs if name == "reduce2" else seqs)
         return pltpu.make_async_remote_copy(
             src_ref=source, dst_ref=target,
             send_sem=y_send.at[group + (index if send_index is None else send_index)],
@@ -537,43 +547,54 @@
         gather_wait("gather2", res_all, "corner", j)
         norm_into(res_all, ffn_gain_ref, normed_ffn, j * SEQ, j * SEQ)
 
-    def ffn(b):
+    def ffn(b, count):
         group = FFN_ROWS * SEQ
-        weight = w_ffn.at[:, pl.ds(b * pair_width, pair_width)]
+        weight = w_ffn.at[:, pl.ds(b * pair_width, count * pair_width)]
 
         @pl.loop(0, rows // group)
         def _(j):
             part = own_rows(group, j)
             both = jnp.dot(normed_ffn[part, :], weight[...], preferred_element_type=f32)
-            hidden[part, b * LANES : (b + 1) * LANES] = (
-                jax.nn.silu(both[:, :LANES]) * both[:, LANES:]
-            ).astype(bf16)
+            for i in range(count):
+                first = i * pair_width
+                hidden[part, (b + i) * LANES : (b + i + 1) * LANES] = (
+                    jax.nn.silu(both[:, first : first + LANES]) * both[:, first + LANES : first + pair_width]
+                ).astype(bf16)
 
     def reduce2(leg, c, j, source, target):
         part = own_rows(SEQ, j)
-        slot = (c % 2) * seqs + j
+        slot = (c % 2 if c + 1 < down_chunks else 2) * seqs + j
         return reduce_copy("reduce2", leg, c * seqs + j, source.at[c, part, :], target.at[c, part, :], slot)
 
+    def keep_far(c, j, corner, across):
+        part = own_rows(SEQ, j)
+        corner2[c, part, :] = corner.astype(bf16)
+        reduce2("corner", c, j, corner2, corner2_in).start()
+        far2[part, :] = across
+
+    def keep_near(c, j, beside, own):
+        part = own_rows(SEQ, j)
+        beside2[c, part, :] = beside.astype(bf16)
+        reduce2("beside", c, j, beside2, beside2_in).start()
+        own2[c, part, :] = own
+
     def down_products(c, j):
-        part = own_rows(SEQ, j)
-        if c + 1 < down_chunks:
-            sums[...] = jnp.dot(hidden[part, :], w_down[c], preferred_element_type=f32)
-        else:
-            sums[...] = begun[part, :] + jnp.dot(
-                hidden[part, split:], w_down[c, split:, :], preferred_element_type=f32
-            )
-        corner2[c, part, :] = sums[:, own_rows(LANES, corner_id)].astype(bf16)
-        reduce2("corner", c, j, corner2, corner2_in).start()
-        beside2[c, part, :] = sums[:, own_rows(LANES, beside_id)].astype(bf16)
-        reduce2("beside", c, j, beside2, beside2_in).start()
-        far2[part, :] = sums[:, own_rows(LANES, across_id)]
-        own2[c, part, :] = sums[:, own_rows(LANES, tp)]
-
-    def down_begin(c):
+        sums[...] = jnp.dot(hidden[own_rows(SEQ, j), :], w_down[c], preferred_element_type=f32)
+        keep_far(c, j, sums[:, own_rows(LANES, corner_id)], sums[:, own_rows(LANES, across_id)])
+        keep_near(c, j, sums[:, own_rows(LANES, beside_id)], sums[:, own_rows(LANES, tp)])
+
+    def pair_products(c, j, which):
+        weight = w_down[c, :, own_rows(pair_width, which)]
+        sums[:, :pair_width] = jnp.dot(hidden[own_rows(SEQ, j), :], weight, preferred_element_type=f32)
+        return sums[:, own_rows(LANES, 1 - core)], sums[:, own_rows(LANES, core)]
+
+    def far_products(c, j):
+        keep_far(c, j, *pair_products(c, j, 1 - chip))
+
+    def down_near(c):
         @pl.loop(0, seqs)
         def _(j):
-            part = own_rows(SEQ, j)
-            begun[part, :] = jnp.dot(hidden[part, :split], w_down[c, :split, :], preferred_element_type=f32)
+            keep_near(c, j, *pair_products(c, j, chip))
 
     def down_onward(c, j):
         part = own_rows(SEQ, j)
@@ -591,12 +612,12 @@
         def _(j):
             down_onward(c, j)
 
-    def down_last(c):
+    def down_piped(c, products):
         @pl.loop(0, seqs + 1)
         def _(j):
             @pl.when(j < seqs)
             def _():
-                down_products(c, j)
+                products(c, j)
 
             @pl.when(j > 0)
             def _():
@@ -645,21 +666,22 @@
 
     at(base + min(r for _, _, r, *_ in PLAN), finish_gather)
     slot = base + 1 + max(n for *_, n in PLAN)
-    for block in range(ffn_blocks):
-        slot = max(slot, 3 * (first_ffn + block + 3) + 2)
-        at(slot, ffn, block)
-        slot += 1 if slot % 3 != FFN_PER_STEP - 1 else 4 - FFN_PER_STEP
+    for block in range(0, ffn_blocks, FFN_BLOCKS):
+        count = min(FFN_BLOCKS, ffn_blocks - block)
+        slot = max(slot, 3 * (first_ffn + block + count - 1 + 3) + 2)
+        at(slot, ffn, block, count)
+        slot += FFN_STRIDE
     for c in range(down_chunks - 1):
-        complete = 3 * (first_down + 3 + c) + 2
+        complete = complete_at(first_down + c)
         if c + 2 < down_chunks:
             at(complete, down, c)
             at(complete + 1, down_rest, c)
+            if c + 3 < down_chunks:
+                at(3 * (first_down + c + 5), finish_down, c)
         else:
-            at(complete, down_last, c)
-        if c + 2 < down_chunks:
-            at(complete + 5, finish_down, c)
-    last_slot = 3 * (total + 3) - 1
-    at(last_slot - 3, down_begin, down_chunks - 1)
+            at(complete, down_piped, c, down_products)
+    last = down_chunks - 1
+    at(complete_at(total - 2), down_piped, last, far_products)
 
     def send_tokens():
         bring_tokens.wait()
@@ -667,13 +689,14 @@
             gather_send("gather1", x_all, "across", j)
             gather_send("gather1", x_all, "beside", j)
 
-    for slot in range(3 * (total + 3)):
+    for slot in range(complete_at(total - 1) + 1):
         advance(slot // 3, slot % 3 + 1)
         for function, args in work.get(slot, ()):
             function(*args)
-    down_last(down_chunks - 1)
-    finish_down(down_chunks - 2)
-    finish_down(down_chunks - 1)
+    down_near(last)
+    finish_down(last - 2)
+    finish_down(last - 1)
+    finish_down(last)
     for step in sorted(pending):
         finish_sends(step)
     for copy in y_pending:
@@ -738,7 +761,6 @@
             pltpu.VMEM((down_chunks, rows, LANES), f32),
             pltpu.VMEM((rows, LANES), f32),
             pltpu.VMEM((SEQ, 4 * LANES), f32),
-            pltpu.VMEM((rows, 4 * LANES), f32),
             pltpu.VMEM((down_chunks, rows, LANES), bf16),
         ]
         + [
@@ -747,7 +769,7 @@
             dma((total, 3)),
             dma((3, 2, 3)),
             dma((total, 3)),
-            dma((12 * seqs,)),
+            dma((15 * seqs,)),
             dma((9 * seqs + 3 * seqs * down_chunks,)),
             dma((down_chunks,)),
         ],

time: 203 us -> 202 us (level)
  no operation moved by 1% of the time
where the time goes in v3:
time: 202 us
  Pallas kernels  199 us (99%)
  local copies, waits for them, and re-layouts  2.26 us (1%)
    pallas_call x1, Pallas kernels, layer(): pl.pallas_call(fused_kernel, out_shape=jax.ShapeDtypeStruct((rows, width)...  199 us

profile of v3, /device:TPU:0, one launch (start us, length us, event | category | flops | bytes accessed | tf_op | source)
XLA Modules:
  0.0 201.6 jit_solution(13836068705997252545)
XLA Ops:
  0.0 199.3 %layer.1 = bf16[1024,512]{1,0:T(8,128)(2,1)} custom-call(bf16[1024,512]{1,0:T(8,128)(2,1)} %tokens_ref.1, f32[1,2048]{1,0:T(1,128)} %bitcast.2, bf16[512,128]{1,0:T(8,128)(2,1)} %query_ref.1, bf16[512,128]{1,0:T(8,128)(2,1)} %key_ref.1, bf16[512,256]{1,0:T(8,128)(2,1)} %value_ref.1, bf16[512,256]{1,0:T(8,128)(2,1)} %gate_ref.1, ...), custom_call_target="tpu_custom_call" | custom-call | tf_op jit(solution)/shard_map/layer/pallas_call | solution.py:732
  199.3 2.3 %copy.17 = bf16[1024,512]{1,0:T(8,128)(2,1)} copy(bf16[1024,512]{1,0:T(8,128)(2,1)} %layer.1) | data formatting | bytes 2097152
